TPU v7x, 32 devices: a whole 2x2x4 slice. The times are simulated.
32 devices in a mesh: sp: 4 (over z), fs: 4 (over y, x), tp: 2 (over core).
Axes of the slice: x: 2, y: 2, z: 4, core: 2. Of those that a mesh axis runs over, the one named last changes fastest.
Arguments:
- tokens: bfloat16 [4, 512, 4096], P('fs', 'sp'), may hold values from -6 to 6
- norm_gain: float32 [4096], replicated, may hold values from 0.1 to 1.9
- pool_proj: bfloat16 [4096, 1024], P(('sp', 'fs'), 'tp'), may hold values from -0.09375 to 0.09375
- query_proj: bfloat16 [4096, 1024], P(('sp', 'fs'), 'tp'), may hold values from -0.09375 to 0.09375
- key_proj: bfloat16 [4096, 1024], P(('sp', 'fs'), 'tp'), may hold values from -0.09375 to 0.09375
- value_proj: bfloat16 [4096, 1024], P(('sp', 'fs'), 'tp'), may hold values from -0.09375 to 0.09375
- pool_map: bfloat16 [4, 256, 256], replicated, may hold values from -0.375 to 0.375
- pool_scale: float32 [1024], replicated, may hold values from 0.1 to 1.9
- decay_rate: float32 [4], P('tp'), may hold values from 2e-05 to 0.034
- start_state: float32 [4, 4, 256, 256], P('fs', 'tp', 'sp'), may hold values from -96 to 96
- pool_back: bfloat16 [1024, 4096], P('tp', ('sp', 'fs')), may hold values from -0.125 to 0.125
- retention_back: bfloat16 [1024, 4096], P('tp', ('sp', 'fs')), may hold values from -0.125 to 0.125
Outputs:
- mixed: bfloat16 [4, 512, 4096], P('fs', ('sp', 'tp'))
All inputs are finite; a program needn't handle non-finite values.
Results may differ from a plain program's by a relative error of at most 0.014.
Values may be sent and summed in bfloat16 or wider, within the bound.
A program may use at most 128 MiB of HBM per device.

v0:
```python
import jax
import jax.numpy as jnp
from jax import lax
from jax.sharding import PartitionSpec as P

GROUPS = 4
BLOCK = 128
HALO = 16
eps = 1e-06
rope_base = 10000.0
highest_precision = lax.Precision.HIGHEST
window_list = (2, 4, 8, 16)


def shortened(x):
    return jax.tree.map(lambda a: a.astype(jnp.bfloat16) if a.dtype == jnp.float32 else a, x)


def shifted(x, axis, by):
    devices = lax.axis_size(axis)
    pairs = [(i, i + by) for i in range(devices) if 0 <= i + by < devices]
    return lax.ppermute(x, axis, pairs)


def carried_in(value, axis, join, neutral):
    count, mine = (lax.axis_size(axis), lax.axis_index(axis))
    pieces = jax.tree.map(lambda part: lax.all_gather(part, axis), value)
    running = jax.tree.map(
        lambda part, zero: jnp.full_like(part, 0) + jnp.asarray(zero, part.dtype), value, neutral
    )

    def turn(position, running):
        longer = join(running, jax.tree.map(lambda part: part[position], pieces))
        return jax.tree.map(lambda new, old: jnp.where(position < mine, new, old), longer, running)

    return lax.fori_loop(0, count - 1, turn, running)


def rotate(values, positions):
    half_dim = values.shape[-1] // 2
    inv_freq = 1.0 / rope_base ** jnp.linspace(0.0, 1.0, half_dim, dtype=jnp.float32)
    angles = positions.astype(jnp.float32)[:, None] * inv_freq[None, :]
    cosine = jnp.cos(angles)[:, None, :]
    sine = jnp.sin(angles)[:, None, :]
    first_half = values[..., :half_dim]
    second_half = values[..., half_dim:]
    return jnp.concatenate(
        [first_half * cosine - second_half * sine, first_half * sine + second_half * cosine],
        axis=-1,
    )


def trailing_sums(extended, length):
    begin = extended.shape[0] - length
    running = extended[begin:]
    results = []
    for behind in range(1, 16):
        running = running + extended[begin - behind : begin - behind + length]
        if behind + 1 in window_list:
            results.append(running)
    return results


def reshape_blocks(array):
    return array.reshape((array.shape[0] // BLOCK, BLOCK) + array.shape[1:])


def block_retention(queries, keys_in, values_in, decay_rate, initial):
    length, head_count, head_dim = queries.shape
    within = jnp.arange(BLOCK, dtype=jnp.float32)
    distance = within[:, None] - within[None, :]
    decay_mask = jnp.where(
        distance[None] >= 0,
        jnp.exp(-jnp.maximum(distance, 0.0)[None] * decay_rate[:, None, None]),
        0.0,
    )
    query_decay_factor = jnp.exp(-(within + 1.0)[:, None] * decay_rate[None, :])
    key_decay_factor = jnp.exp(-(BLOCK - 1.0 - within)[:, None] * decay_rate[None, :])
    block_decay_factor = jnp.exp(-BLOCK * decay_rate)

    def advance(state_carry, inputs):
        block_queries, block_keys, block_values = inputs
        scores = (
            jnp.einsum("ihk,jhk->hij", block_queries, block_keys, precision=highest_precision)
            * decay_mask
        )
        inside = jnp.einsum("hij,jhv->ihv", scores, block_values, precision=highest_precision)
        across_blocks = jnp.einsum(
            "bzy,zyx->bzx",
            block_queries * query_decay_factor[:, :, None],
            state_carry,
            precision=highest_precision,
        )
        state_carry = state_carry * block_decay_factor[:, None, None] + jnp.einsum(
            "flm,fld->lmd",
            block_keys * key_decay_factor[:, :, None],
            block_values,
            precision=highest_precision,
        )
        return (state_carry, inside + across_blocks)

    final_state, outputs = lax.scan(
        advance,
        initial,
        (reshape_blocks(queries), reshape_blocks(keys_in), reshape_blocks(values_in)),
    )
    return (outputs.reshape(length, head_count, values_in.shape[-1]), final_state)


def combine_states(earlier, latter):
    return (earlier[0] * latter[0], latter[0][:, None, None] * earlier[1] + latter[1])


def on_device(
    tokens,
    norm_gain,
    pool_proj,
    query_proj,
    key_proj,
    value_proj,
    pool_map,
    pool_scale,
    decay_rate,
    start_state,
    pool_back,
    retention_back,
):
    sequence = tokens[0]
    length = sequence.shape[0]
    tp_index = lax.axis_index("tp")
    sp_index = lax.axis_index("sp")
    tp_count = lax.axis_size("tp")
    floats = sequence.astype(jnp.float32)
    normed = (
        floats * lax.rsqrt(jnp.mean(floats * floats, axis=-1, keepdims=True) + eps) * norm_gain
    ).astype(jnp.bfloat16)
    group_normed = lax.all_gather(normed, "fs", axis=0, tiled=True)
    quarters = (
        lax.all_to_all(pool_proj, "fs", split_axis=1, concat_axis=0, tiled=True),
        lax.all_to_all(query_proj, "fs", split_axis=1, concat_axis=0, tiled=True),
        lax.all_to_all(key_proj, "fs", split_axis=1, concat_axis=0, tiled=True),
        lax.all_to_all(value_proj, "fs", split_axis=1, concat_axis=0, tiled=True),
    )
    pieces = (
        lax.all_gather(quarters[0], "sp", axis=0, tiled=True),
        lax.all_gather(quarters[1], "sp", axis=0, tiled=True),
        lax.all_gather(quarters[2], "sp", axis=0, tiled=True),
        lax.all_gather(quarters[3], "sp", axis=0, tiled=True),
    )
    partial_cols = tuple(
        (jnp.dot(group_normed, piece_w, preferred_element_type=jnp.float32) for piece_w in pieces)
    )
    rounded = tuple((result.astype(jnp.bfloat16) for result in partial_cols))
    pool_in, query_bf, key_bf, value_bf = jax.tree.map(
        lambda part, own: part.astype(own.dtype),
        lax.all_to_all(shortened(rounded), "fs", split_axis=0, concat_axis=1, tiled=True),
        rounded,
    )
    positions = jnp.arange(length, dtype=jnp.int32) + sp_index * length
    before = shifted(pool_in[length - HALO :], "sp", 1)
    extended = jnp.concatenate([before, pool_in], axis=0).astype(jnp.float32)
    stacked = jnp.stack(trailing_sums(extended, length))
    local_groups = GROUPS // tp_count
    channels = pool_in.shape[1]
    group_dim = channels // local_groups
    group_maps = lax.dynamic_slice_in_dim(pool_map, tp_index * local_groups, local_groups, 0)
    scales = lax.dynamic_slice_in_dim(pool_scale, tp_index * channels, channels, 0)
    windows = jnp.array(window_list, dtype=jnp.int32)
    pieces = []
    for group_idx in range(local_groups):
        chosen_group = tp_index * local_groups + group_idx
        lower = group_idx * group_dim
        chosen = lax.dynamic_index_in_dim(stacked, chosen_group, 0, keepdims=False)[
            :, lower : lower + group_dim
        ]
        counts = jnp.minimum(windows[chosen_group], positions + 1).astype(jnp.float32)
        inputs = extended[HALO:, lower : lower + group_dim]
        differ = (chosen / counts[:, None] - inputs).astype(jnp.bfloat16)
        pieces.append(jnp.dot(differ, group_maps[group_idx], preferred_element_type=jnp.float32))
    pool_out = (jnp.concatenate(pieces, axis=1) * scales).astype(jnp.bfloat16)
    head_count = decay_rate.shape[0]
    head_dim = query_bf.shape[1] // head_count
    queries = rotate(query_bf.astype(jnp.float32).reshape(length, head_count, head_dim), positions)
    keys_in = rotate(
        key_bf.astype(jnp.float32).reshape(length, head_count, head_dim), positions
    ) * head_dim ** (-0.5)
    values_in = value_bf.astype(jnp.float32).reshape(length, head_count, head_dim)
    zeros_state = jnp.zeros((head_count, head_dim, head_dim), jnp.float32)
    local_output, local_state = block_retention(
        queries, keys_in, values_in, decay_rate, zeros_state
    )
    span_decay = jnp.exp(-decay_rate * length)
    whole_start = lax.all_gather(start_state, "sp", axis=2, tiled=True)[0]
    span_factor, carried_over = carried_in(
        (span_decay, local_state), "sp", combine_states, (jnp.ones_like(span_decay), zeros_state)
    )
    offset_float = (sp_index * length).astype(jnp.float32)
    carried_over = carried_over + jnp.exp(-decay_rate * offset_float)[:, None, None] * whole_start
    steps_in = jnp.arange(length, dtype=jnp.float32) + 1.0
    query_rows_scaled = queries * jnp.exp(-steps_in[:, None] * decay_rate[None, :])[:, :, None]
    retained_output = local_output + jnp.einsum(
        "lpi,pib->lpb", query_rows_scaled, carried_over, precision=highest_precision
    )
    retained_output = retained_output * lax.rsqrt(
        jnp.mean(retained_output * retained_output, axis=-1, keepdims=True) + eps
    )
    ret_out = retained_output.reshape(length, head_count * head_dim).astype(jnp.bfloat16)
    pool_cols, retention_cols = (
        lax.all_gather(pool_back, ("sp", "fs"), axis=1, tiled=True),
        lax.all_gather(retention_back, ("sp", "fs"), axis=1, tiled=True),
    )
    weight_local = jnp.concatenate([pool_cols, retention_cols], axis=0)
    joined = jnp.concatenate([pool_out, ret_out], axis=1)
    mixed = lax.psum_scatter(
        jnp.dot(joined, weight_local, preferred_element_type=jnp.float32).astype(jnp.bfloat16),
        "tp",
        scatter_dimension=0,
        tiled=True,
    )
    return mixed[None]


def solution(mesh):
    placed = (
        P("fs", "sp", None),
        P(),
        P(("sp", "fs"), "tp"),
        P(("sp", "fs"), "tp"),
        P(("sp", "fs"), "tp"),
        P(("sp", "fs"), "tp"),
        P(),
        P(),
        P("tp"),
        P("fs", "tp", "sp", None),
        P("tp", ("sp", "fs")),
        P("tp", ("sp", "fs")),
    )
    return jax.shard_map(
        on_device,
        mesh=mesh,
        in_specs=placed,
        out_specs=P("fs", ("sp", "tp"), None),
        check_vma=False,
    )
```

profile of v0, /device:TPU:0, one launch (start us, length us, event | category | flops | bytes accessed | tf_op | source)
XLA Modules:
  0.0 432.0 jit_solution(100196734017617633)
XLA Ops:
  6.5 1.2 copy.58
  7.7 10.7 %all_to_all.137 = bf16[256,4,128]{0,2,1:T(8,128)(2,1)S(1)} all-to-all(bf16[256,4,128]{0,2,1:T(8,128)(2,1)S(1)} %bitcast.100), channel_id=1, replica_groups=mesh['sp'=4,'fs'=4,'tp'=2] {'fs'}, dimensions={1} | all-to-all | bytes 524288 | tf_op jit(solution)/shard_map/all_to_all | solution.py:140
  18.4 0.9 copy.59
  19.4 1.5 fusion.8
  20.9 2.6 fusion.10
  23.7 8.1 %all_to_all.138 = bf16[256,4,128]{0,2,1:T(8,128)(2,1)S(1)} all-to-all(bf16[256,4,128]{0,2,1:T(8,128)(2,1)S(1)} %bitcast.101), channel_id=1, replica_groups=mesh['sp'=4,'fs'=4,'tp'=2] {'fs'}, dimensions={1} | all-to-all | bytes 524288 | tf_op jit(solution)/shard_map/all_to_all | solution.py:141
  31.9 0.8 copy.64
  32.9 8.1 %all_to_all.139 = bf16[256,4,128]{0,2,1:T(8,128)(2,1)S(1)} all-to-all(bf16[256,4,128]{0,2,1:T(8,128)(2,1)S(1)} %bitcast.102), channel_id=1, replica_groups=mesh['sp'=4,'fs'=4,'tp'=2] {'fs'}, dimensions={1} | all-to-all | bytes 524288 | tf_op jit(solution)/shard_map/all_to_all | solution.py:142
  41.0 0.8 copy.56
  41.9 0.8 copy.50
  42.8 3.4 all-to-all-start
  48.0 3.5 all-to-all-done
  51.5 0.9 copy.51
  52.4 48.6 %all-gather.11.cloned.1.call-done = bf16[512,4096]{1,0:T(8,128)(2,1)} async-done(((bf16[128,4096]{1,0:T(8,128)(2,1)}), bf16[512,4096]{1,0:T(8,128)(2,1)}) %all-gather.11.cloned.1.call-update) | async-done | bytes 4194320 | tf_op jit(solution)/shard_map/all_gather | solution.py:137
  101.0 3.7 convolution_convert_fusion.1
  104.7 0.8 copy.60
  105.5 3.3 all-to-all-start.5
  108.8 21.8 %all-gather.19.cloned.1.call-done = bf16[4096,128]{1,0:T(8,128)(2,1)} async-done(((bf16[1024,128]{1,0:T(8,128)(2,1)}), bf16[4096,128]{1,0:T(8,128)(2,1)}) %all-gather.19.cloned.1.call-update) | async-done | bytes 1048592 | tf_op jit(solution)/shard_map/all_gather | solution.py:147
  130.6 3.7 convolution_convert_fusion
  134.3 0.8 copy.65
  135.1 3.7 all-to-all-start.7
  138.7 20.7 %all-gather.15.cloned.1.call-done = bf16[4096,128]{1,0:T(8,128)(2,1)} async-done(((bf16[1024,128]{1,0:T(8,128)(2,1)}), bf16[4096,128]{1,0:T(8,128)(2,1)}) %all-gather.15.cloned.1.call-update) | async-done | bytes 1048592 | tf_op jit(solution)/shard_map/all_gather | solution.py:148
  159.4 4.4 %convolution_convert_fusion.2 = bf16[512,128]{1,0:T(8,128)(2,1)} fusion(bf16[512,4096]{1,0:T(8,128)(2,1)} %all-gather.11.cloned.1.call-done, bf16[4096,128]{1,0:T(8,128)(2,1)} %all-gather.15.cloned.1.call-done), kind=kOutput, calls=%fused_computation.19 | convolution fusion | flops 536936448 | bytes 5373952 | tf_op jit(solution)/shard_map/dot_general | solution.py:151
  163.8 3.8 all-to-all-start.3
  168.1 4.5 %all-to-all-done.3 = bf16[4,128,128]{2,1,0:T(8,128)(2,1)S(1)} async-done(((bf16[4,128,128]{2,1,0:T(8,128)(2,1)}), bf16[4,128,128]{2,1,0:T(8,128)(2,1)S(1)}, u32[]{:S(2)}, u32[]{:S(2)}) %all-to-all-start.3) | async-done | bytes 131104 | tf_op jit(solution)/shard_map/all_to_all | solution.py:156
  172.9 1.3 convolution_add_fusion
  174.2 0.7 all-gather.21.cloned.1.call-update
  175.0 0.7 all-gather.23.cloned.1.call-update
  175.7 10.7 %all-reduce = f32[8]{0:T(128)S(1)} all-reduce(f32[8]{0:T(128)S(1)} %get-tuple-element.181), channel_id=2, replica_groups=mesh['sp'=4,'fs'=4,'tp'=2] {'sp'}, use_global_device_ids=true, to_apply=%add | all-reduce | flops 8 | bytes 64
  187.2 14.7 %all_gather.45 = f32[1,2,256,256]{3,2,1,0:T(8,128)S(1)} all-gather(f32[1,2,64,256]{3,2,1,0:T(8,128)S(1)} %copy-done.4), channel_id=1, replica_groups=mesh['sp'=4,'fs'=4,'tp'=2] {'sp'}, dimensions={2}, use_global_device_ids=true | all-gather | bytes 655360 | tf_op jit(solution)/shard_map/all_gather | solution.py:193
  201.9 3.7 convolution_convert_fusion.3
  205.6 0.8 copy.52
  206.4 3.3 all-to-all-start.1
  209.8 1.3 minimum_convert_fusion
  211.1 3.7 all-to-all-done.1
  214.9 3.1 collective-permute-start
  218.7 0.7 convolution_add_fusion.2
  219.8 1.1 fusion.14
  221.7 14.9 %all-gather.25.cloned.1.call-done = f32[8,256,256]{2,1,0:T(8,128)} async-done(((f32[2,256,256]{2,1,0:T(8,128)}), f32[8,256,256]{2,1,0:T(8,128)}) %all-gather.25.cloned.1.call-update) | async-done | bytes 2097168 | tf_op jit(solution)/shard_map/all_gather | solution.py:27
  236.6 3.6 while.9
  236.6 1.2 fusion.67
  237.8 1.2 fusion.67
  239.0 1.2 fusion.67
  240.2 1.2 multiply_reduce_fusion
  241.5 83.7 %all-gather.21.cloned.1.call-done = bf16[512,4096]{1,0:T(8,128)(2,1)} async-done(((bf16[512,256]{1,0:T(8,128)(2,1)}), bf16[512,4096]{1,0:T(8,128)(2,1)}) %all-gather.21.cloned.1.call-update) | async-done | bytes 4194320 | tf_op jit(solution)/shard_map/all_gather | solution.py:209
  325.2 87.7 %all-gather.23.cloned.1.call-done = bf16[512,4096]{1,0:T(8,128)(2,1)} async-done(((bf16[512,256]{1,0:T(8,128)(2,1)}), bf16[512,4096]{1,0:T(8,128)(2,1)}) %all-gather.23.cloned.1.call-update) | async-done | bytes 4194320 | tf_op jit(solution)/shard_map/all_gather | solution.py:210
  412.9 5.8 %fusion.5 = bf16[128,4096]{1,0:T(8,128)(2,1)} fusion(bf16[512,4096]{1,0:T(8,128)(2,1)} %all-gather.23.cloned.1.call-done, bf16[512,4096]{1,0:T(8,128)(2,1)} %all-gather.21.cloned.1.call-done, bf16[128,512]{1,0:T(8,128)(2,1)S(1)} %copy.76, bf16[128,512]{1,0:T(8,128)(2,1)S(1)} %fusion.15), kind=kOutput, calls=%fused_computation.7 | convolution fusion | flops 1091567616 | bytes 9699328 | tf_op jit(solution)/shard_map/dot_general | solution.py:215
  418.8 6.7 %reduce-scatter.2.cloned.1.call-done = bf16[64,4096]{1,0:T(8,128)(2,1)} async-done(((bf16[128,4096]{1,0:T(8,128)(2,1)}), bf16[64,4096]{1,0:T(8,128)(2,1)}) %reduce-scatter.2.cloned.1.call-update) | async-done | bytes 524304 | tf_op jit(solution)/shard_map/reduce_scatter | solution.py:214
  (84 shorter events, 5.6 us)
Async XLA Ops:
  6.5 214.6 %copy-start = (bf16[4,256,256]{2,1,0:T(8,128)(2,1)S(1)}, bf16[4,256,256]{2,1,0:T(8,128)(2,1)}, u32[]{:S(2)}) copy-start(bf16[4,256,256]{2,1,0:T(8,128)(2,1)} %param.23) | copy-start | bytes 1572868
  6.5 17.1 %copy-start.1 = (bf16[256,512]{1,0:T(8,128)(2,1)S(1)}, bf16[256,512]{1,0:T(8,128)(2,1)}, u32[]{:S(2)}) copy-start(bf16[256,512]{1,0:T(8,128)(2,1)} %param.21) | copy-start | bytes 786436
  6.5 26.2 %copy-start.2 = (bf16[256,512]{1,0:T(8,128)(2,1)S(1)}, bf16[256,512]{1,0:T(8,128)(2,1)}, u32[]{:S(2)}) copy-start(bf16[256,512]{1,0:T(8,128)(2,1)} %param.22) | copy-start | bytes 786436
  6.5 45.9 %all-gather.17.cloned.1.call-start = ((), (), s32[]{:S(2)}) async-start(), calls=%async_computation.12 | async-start | bytes 1310720 | tf_op jit(solution)/shard_map/all_gather | solution.py:146
  19.3 22.6 %copy-start.3 = (bf16[256,512]{1,0:T(8,128)(2,1)S(1)}, bf16[256,512]{1,0:T(8,128)(2,1)}, u32[]{:S(2)}) copy-start(bf16[256,512]{1,0:T(8,128)(2,1)} %param.19) | copy-start | bytes 786436
  19.3 81.7 %all-gather.11.cloned.1.call-start = ((), (), s32[]{:S(2)}) async-start(), calls=%async_computation.9 | async-start | bytes 5242880 | tf_op jit(solution)/shard_map/all_gather | solution.py:137
  20.9 25.3 %copy-start.8 = (u32[32]{0:T(128)S(1)}, u32[32]{0:T(128)}, u32[]{:S(2)}) copy-start(u32[32]{0:T(128)} %constant.104) | copy-start | bytes 388
  20.9 26.6 %copy-start.5 = (f32[2]{0:T(128)S(1)}, f32[2]{0:T(128)}, u32[]{:S(2)}) copy-start(f32[2]{0:T(128)} %param.25) | copy-start | bytes 28
  23.5 107.0 %all-gather.19.cloned.1.call-start = ((), (), s32[]{:S(2)}) async-start(), calls=%async_computation.13 | async-start | bytes 1310720 | tf_op jit(solution)/shard_map/all_gather | solution.py:147
  32.7 126.7 %all-gather.15.cloned.1.call-start = ((), (), s32[]{:S(2)}) async-start(), calls=%async_computation.11 | async-start | bytes 1310720 | tf_op jit(solution)/shard_map/all_gather | solution.py:148
  42.8 8.8 %all-to-all-start = ((bf16[256,4,128]{0,2,1:T(8,128)(2,1)}), bf16[256,4,128]{0,2,1:T(8,128)(2,1)S(1)}, u32[]{:S(2)}, u32[]{:S(2)}) async-start(bf16[256,4,128]{0,2,1:T(8,128)(2,1)} %bitcast.2), calls=%async_computation | async-start | bytes 524288 | tf_op jit(solution)/shard_map/all_to_all | solution.py:139
  46.2 155.7 %all-gather.13.cloned.1.call-start = ((), (), s32[]{:S(2)}) async-start(), calls=%async_computation.10 | async-start | bytes 1310720 | tf_op jit(solution)/shard_map/all_gather | solution.py:145
  105.5 29.6 %all-to-all-start.5 = ((bf16[4,128,128]{1,2,0:T(8,128)(2,1)}), bf16[4,128,128]{1,2,0:T(8,128)(2,1)S(1)}, u32[]{:S(2)}, u32[]{:S(2)}) async-start(bf16[4,128,128]{1,2,0:T(8,128)(2,1)} %copy.60), calls=%async_computation.5 | async-start | bytes 262144 | tf_op jit(solution)/shard_map/all_to_all | solution.py:156
  135.1 28.7 %all-to-all-start.7 = ((bf16[4,128,128]{1,2,0:T(8,128)(2,1)}), bf16[4,128,128]{1,2,0:T(8,128)(2,1)S(1)}, u32[]{:S(2)}, u32[]{:S(2)}) async-start(bf16[4,128,128]{1,2,0:T(8,128)(2,1)} %copy.65), calls=%async_computation.7 | async-start | bytes 262144 | tf_op jit(solution)/shard_map/all_to_all | solution.py:156
  163.8 22.6 %copy-start.7 = (f32[1024]{0:T(1024)S(1)}, f32[1024]{0:T(1024)}, u32[]{:S(2)}) copy-start(f32[1024]{0:T(1024)} %param.24) | copy-start | bytes 12292
  163.8 22.7 %copy-start.6 = (s32[4]{0:T(128)S(1)}, s32[4]{0:T(128)}, u32[]{:S(2)}) copy-start(s32[4]{0:T(128)} %constant.99.clone) | copy-start | bytes 52
  163.8 23.4 %copy-start.4 = (f32[1,2,64,256]{3,2,1,0:T(8,128)S(1)}, f32[1,2,64,256]{3,2,1,0:T(8,128)}, u32[]{:S(2)}) copy-start(f32[1,2,64,256]{3,2,1,0:T(8,128)} %param.26) | copy-start | bytes 393220
  163.8 8.8 %all-to-all-start.3 = ((bf16[4,128,128]{2,1,0:T(8,128)(2,1)}), bf16[4,128,128]{2,1,0:T(8,128)(2,1)S(1)}, u32[]{:S(2)}, u32[]{:S(2)}) async-start(bf16[4,128,128]{2,1,0:T(8,128)(2,1)} %bitcast.22), calls=%async_computation.3 | async-start | bytes 262144 | tf_op jit(solution)/shard_map/all_to_all | solution.py:156
  167.6 69.0 %all-gather.25.cloned.1.call-start = ((), (), s32[]{:S(2)}) async-start(), calls=%async_computation.17 | async-start | bytes 2621440 | tf_op jit(solution)/shard_map/all_gather | solution.py:27
  174.2 151.0 %all-gather.21.cloned.1.call-start = ((), (), s32[]{:S(2)}) async-start(), calls=%async_computation.14 | async-start | bytes 4456448 | tf_op jit(solution)/shard_map/all_gather | solution.py:209
  174.9 238.0 %all-gather.23.cloned.1.call-start = ((), (), s32[]{:S(2)}) async-start(), calls=%async_computation.15 | async-start | bytes 4456448 | tf_op jit(solution)/shard_map/all_gather | solution.py:210
  206.4 8.3 %all-to-all-start.1 = ((bf16[4,128,128]{1,2,0:T(8,128)(2,1)}), bf16[4,128,128]{1,2,0:T(8,128)(2,1)S(1)}, u32[]{:S(2)}, u32[]{:S(2)}) async-start(bf16[4,128,128]{1,2,0:T(8,128)(2,1)} %copy.52), calls=%async_computation.1 | async-start | bytes 262144 | tf_op jit(solution)/shard_map/all_to_all | solution.py:156
  209.7 215.7 %reduce-scatter.2.cloned.1.call-start = ((), (), s32[]{:S(2)}) async-start(), calls=%async_computation.16 | async-start | bytes 1572864 | tf_op jit(solution)/shard_map/reduce_scatter | solution.py:214
  214.9 4.6 %collective-permute-start = (bf16[16,512]{1,0:T(8,128)(2,1)S(1)}, bf16[16,512]{1,0:T(8,128)(2,1)S(1)}, u32[]{:S(2)}, u32[]{:S(2)}) collective-permute-start(bf16[16,512]{1,0:T(8,128)(2,1)S(1)} %copy.75), channel_id=1, source_target_pairs={{0,8},{8,16},{16,24},{1,9},{9,17},{17,25},{2,10},{10,18},{18,26},{... | collective-permute-start | bytes 49160 | tf_op jit(solution)/shard_map/ppermute | solution.py:22
Sparse Core Ops, SparseCore 0:
  19.4 27.6 all-gather.16
  49.0 51.9 all-gather.10
  102.6 27.9 all-gather.18
  132.0 27.3 all-gather.14
  160.8 28.7 all-gather.12
  191.1 45.4 all-gather.24
  239.3 85.8 all-gather.20
  327.9 84.9 all-gather.22
  418.9 6.5 reduce-scatter.1
where the time goes:
time: 433 us; the launch traced here: 432 us
  waiting for transfers between devices  297 us (69%)
  blocking collectives  52.3 us (12%)
  matrix products  25.7 us (6%)
  starting transfers between devices  20.9 us (5%)
  between operations  14.2 us (3%)
  other arithmetic  11.1 us (3%)
  local copies, waits for them, and re-layouts  10.4 us (2%)
    all_gather x1, waiting for transfers between devices, on_device(): lax.all_gather(retention_back, ('sp', 'fs'), axis=1, tiled=True)  87.7 us
    all_gather x1, waiting for transfers between devices, on_device(): lax.all_gather(pool_back, ('sp', 'fs'), axis=1, tiled=True)  83.7 us
    all_gather x1, waiting for transfers between devices, on_device(): group_normed = lax.all_gather(normed, 'fs', axis=0, tiled=True)  48.6 us
    all_gather x1, waiting for transfers between devices, on_device(): lax.all_gather(quarters[2], 'sp', axis=0, tiled=True)  21.8 us
    all_gather x1, waiting for transfers between devices, on_device(): lax.all_gather(quarters[3], 'sp', axis=0, tiled=True)  20.7 us
    dot_general x4, matrix products, on_device(): jnp.dot(group_normed, piece_w, preferred_element_type=jnp.float32)  15.6 us
    all_gather x1, waiting for transfers between devices, carried_in(): pieces = jax.tree.map(lambda part: lax.all_gather(part, axis), value)  14.9 us
    all_gather x1, blocking collectives, on_device(): whole_start = lax.all_gather(start_state, 'sp', axis=2, tiled=True)[0]  14.7 us
  transfers between devices with their start and end apart: 15, of which 11 were waited for; matrix products, arithmetic and copies ran while one was open for 9% of the time, Pallas kernels for 0%

commit v1 on v0

--- a/solution.py
+++ b/solution.py
@@ -10,6 +10,22 @@
 rope_base = 10000.0
 highest_precision = lax.Precision.HIGHEST
 window_list = (2, 4, 8, 16)
+
+
+def draft_the_row(piece_in):
+    n_parts = lax.axis_size("fs")
+    seen = []
+    for q in [*range(1, n_parts)]:
+        seen.append((q - 1, q))
+    upper = piece_in
+    series = [upper]
+    seen_now = seen + [(n_parts - 1, 0)]
+    for _ in [*range(n_parts - 1)]:
+        upper = lax.ppermute(upper, axis_name="fs", perm=seen_now)
+        series += [upper]
+    even = jnp.concatenate([*reversed(series)], 0)
+    mixed_arr = jnp.roll(even, (lax.axis_index("fs") + 1) * upper.shape[0], 0)
+    return mixed_arr
 
 
 def shortened(x):
@@ -134,7 +150,7 @@
     normed = (
         floats * lax.rsqrt(jnp.mean(floats * floats, axis=-1, keepdims=True) + eps) * norm_gain
     ).astype(jnp.bfloat16)
-    group_normed = lax.all_gather(normed, "fs", axis=0, tiled=True)
+    group_normed = draft_the_row(normed)
     quarters = (
         lax.all_to_all(pool_proj, "fs", split_axis=1, concat_axis=0, tiled=True),
         lax.all_to_all(query_proj, "fs", split_axis=1, concat_axis=0, tiled=True),

time: 433 us -> 411 us (0.949)
  waiting for transfers between devices: 297 us -> 235 us
  blocking collectives: 52.3 us -> 67.8 us
  local copies, waits for them, and re-layouts: 10.4 us -> 24.5 us
  starting transfers between devices: 20.9 us -> 27.9 us
    all_gather x1 -> x0, waiting for transfers between devices: 48.6 us -> none  [on_device(): group_normed = lax.all_gather(normed, 'fs', axis=0, tiled=True)]
    ppermute x0 -> x3, waiting for transfers between devices: none -> 43.5 us  [draft_the_row(): upper = lax.ppermute(upper, axis_name='fs', perm=seen_now)]
    all_gather x1, waiting for transfers between devices: 21.8 us -> 0.01 us  [on_device(): lax.all_gather(quarters[2], 'sp', axis=0, tiled=True)]
    all_gather x1, waiting for transfers between devices: 20.7 us -> 0.01 us  [on_device(): lax.all_gather(quarters[3], 'sp', axis=0, tiled=True)]
    all_to_all x1, blocking collectives: 8.11 us -> 24.4 us  [on_device(): lax.all_to_all(value_proj, 'fs', split_axis=1, concat_axis=0, tiled=True)]
    all_gather x1, waiting for transfers between devices: 14.9 us -> 0.02 us  [carried_in(): pieces = jax.tree.map(lambda part: lax.all_gather(part, axis), value)]
    unnamed x28 -> x34, local copies, waits for them, and re-layouts: 3.29 us -> 17.4 us
    all_to_all x1 -> x0, blocking collectives: 10.7 us -> none  [on_device(): lax.all_to_all(query_proj, 'fs', split_axis=1, concat_axis=0, tiled=True)]
  transfers between devices with their start and end apart: 15 -> 18, of which waited for: 11 -> 10; matrix products, arithmetic and copies ran while one was open for 9% -> 14% of each run, Pallas kernels for 0% -> 0%
where the time goes in v1:
time: 411 us; the launch traced here: 410 us
  waiting for transfers between devices  235 us (57%)
  blocking collectives  67.8 us (16%)
  starting transfers between devices  27.9 us (7%)
  matrix products  25.9 us (6%)
  local copies, waits for them, and re-layouts  24.5 us (6%)
  between operations  14.6 us (4%)
  other arithmetic  13.7 us (3%)
    all_gather x1, waiting for transfers between devices, on_device(): lax.all_gather(retention_back, ('sp', 'fs'), axis=1, tiled=True)  87.7 us
    all_gather x1, waiting for transfers between devices, on_device(): lax.all_gather(pool_back, ('sp', 'fs'), axis=1, tiled=True)  84.3 us
    ppermute x3, waiting for transfers between devices, draft_the_row(): upper = lax.ppermute(upper, axis_name='fs', perm=seen_now)  43.5 us
    all_to_all x1, blocking collectives, on_device(): lax.all_to_all(value_proj, 'fs', split_axis=1, concat_axis=0, tiled=True)  24.4 us
    all_gather x1, blocking collectives, on_device(): whole_start = lax.all_gather(start_state, 'sp', axis=2, tiled=True)[0]  20.4 us
    unnamed x34, local copies, waits for them, and re-layouts  17.4 us
    dot_general x4, matrix products, on_device(): jnp.dot(group_normed, piece_w, preferred_element_type=jnp.float32)  15.6 us
    all_to_all x4, starting transfers between devices, on_device(): lax.all_to_all(shortened(rounded), 'fs', split_axis=0, concat_axis=1, til...  14 us
  transfers between devices with their start and end apart: 18, of which 10 were waited for; matrix products, arithmetic and copies ran while one was open for 14% of the time, Pallas kernels for 0%

profile of v1, /device:TPU:0, one launch (start us, length us, event | category | flops | bytes accessed | tf_op | source)
XLA Modules:
  0.0 409.7 jit_solution(10076306126153238768)
XLA Ops:
  6.6 1.2 copy.63
  7.8 10.8 %all_to_all.137 = bf16[256,4,128]{0,2,1:T(8,128)(2,1)S(1)} all-to-all(bf16[256,4,128]{0,2,1:T(8,128)(2,1)S(1)} %bitcast.100), channel_id=1, replica_groups=mesh['sp'=4,'fs'=4,'tp'=2] {'fs'}, dimensions={1} | all-to-all | bytes 524288 | tf_op jit(solution)/shard_map/all_to_all | solution.py:157
  18.6 0.8 copy.64
  19.5 1.8 copy.58
  21.3 3.4 all-to-all-start.4
  24.8 1.6 fusion.16
  26.3 2.6 fusion.18
  28.9 1.9 collective-permute-start
  31.8 21.8 %collective-permute-done = bf16[128,4096]{1,0:T(8,128)(2,1)S(1)} collective-permute-done((bf16[128,4096]{1,0:T(8,128)(2,1)}, bf16[128,4096]{1,0:T(8,128)(2,1)S(1)}, u32[]{:S(2)}, u32[]{:S(2)}) %collective-permute-start) | collective-permute-done | bytes 1048608 | tf_op jit(solution)/shard_map/ppermute | solution.py:24
  54.4 1.1 copy.55
  55.5 24.4 %all_to_all.138 = bf16[256,4,128]{0,2,1:T(8,128)(2,1)S(1)} all-to-all(bf16[256,4,128]{0,2,1:T(8,128)(2,1)S(1)} %bitcast.101), channel_id=1, replica_groups=mesh['sp'=4,'fs'=4,'tp'=2] {'fs'}, dimensions={1} | all-to-all | bytes 524288 | tf_op jit(solution)/shard_map/all_to_all | solution.py:158
  81.6 3.4 all-to-all-start
  85.1 1.9 collective-permute-start.2
  89.0 2.6 all-to-all-done
  92.4 21.7 %collective-permute-done.2 = bf16[128,4096]{1,0:T(8,128)(2,1)} collective-permute-done((bf16[128,4096]{1,0:T(8,128)(2,1)}, bf16[128,4096]{1,0:T(8,128)(2,1)}, u32[]{:S(2)}, u32[]{:S(2)}) %collective-permute-start.2) | collective-permute-done | bytes 1048608 | tf_op jit(solution)/shard_map/ppermute | solution.py:24
  114.1 2.3 constant_dynamic-update-slice_fusion.7
  116.4 2.4 constant_dynamic-update-slice_fusion.6
  118.8 1.0 constant_dynamic-update-slice_fusion.5
  119.8 1.3 constant_dynamic-update-slice_fusion.4
  121.1 2.3 constant_dynamic-update-slice_fusion.3
  123.4 2.3 constant_dynamic-update-slice_fusion.2
  125.8 1.1 constant_dynamic-update-slice_fusion.1
  126.8 1.4 constant_dynamic-update-slice_fusion
  128.2 3.8 fusion.29
  132.7 3.3 all-to-all-start.7
  136.1 3.8 fusion.26
  141.0 3.8 all-to-all-start.5
  144.8 4.4 %fusion.23 = bf16[512,128]{1,0:T(8,128)(2,1)} fusion(bf16[4096,128]{1,0:T(8,128)(2,1)} %all-gather.12.cloned.1.call-done, bf16[1024,4096]{1,0:T(8,128)(2,1)} %constant_dynamic-update-slice_fusion, s32[]{:T(128)S(6)} %select_n.53), kind=kOutput, calls=%fused_computation.26 | convolution fusion | flops 536936448 | bytes 5373956 | tf_op jit(solution)/shard_map/dot_general | solution.py:167
  149.8 3.6 all-to-all-start.3
  153.9 4.5 %all-to-all-done.3 = bf16[4,128,128]{2,1,0:T(8,128)(2,1)S(1)} async-done(((bf16[4,128,128]{2,1,0:T(8,128)(2,1)}), bf16[4,128,128]{2,1,0:T(8,128)(2,1)S(1)}, u32[]{:S(2)}, u32[]{:S(2)}) %all-to-all-start.3) | async-done | bytes 131104 | tf_op jit(solution)/shard_map/all_to_all | solution.py:172
  158.7 1.3 convolution_add_fusion
  161.3 12.1 %all-reduce = f32[8]{0:T(128)S(1)} all-reduce(f32[8]{0:T(128)S(1)} %get-tuple-element.181), channel_id=2, replica_groups=mesh['sp'=4,'fs'=4,'tp'=2] {'sp'}, use_global_device_ids=true, to_apply=%add | all-reduce | flops 8 | bytes 64
  174.3 20.4 %all_gather.41 = f32[1,2,256,256]{3,2,1,0:T(8,128)S(1)} all-gather(f32[1,2,64,256]{3,2,1,0:T(8,128)S(1)} %copy-done.4), channel_id=1, replica_groups=mesh['sp'=4,'fs'=4,'tp'=2] {'sp'}, dimensions={2}, use_global_device_ids=true | all-gather | bytes 655360 | tf_op jit(solution)/shard_map/all_gather | solution.py:209
  194.7 3.7 fusion.20
  199.2 3.3 all-to-all-start.1
  202.5 1.2 minimum_convert_fusion
  203.7 3.7 all-to-all-done.1
  207.7 2.1 collective-permute-start.3
  211.4 1.1 fusion.34
  213.3 3.6 while.9
  213.4 1.2 fusion.87
  214.6 1.2 fusion.87
  215.8 1.2 fusion.87
  217.0 1.2 multiply_reduce_fusion
  218.3 84.3 %all-gather.18.cloned.1.call-done = bf16[512,4096]{1,0:T(8,128)(2,1)} async-done(((bf16[512,256]{1,0:T(8,128)(2,1)}), bf16[512,4096]{1,0:T(8,128)(2,1)}) %all-gather.18.cloned.1.call-update) | async-done | bytes 4194320 | tf_op jit(solution)/shard_map/all_gather | solution.py:225
  302.6 87.7 %all-gather.20.cloned.1.call-done = bf16[512,4096]{1,0:T(8,128)(2,1)} async-done(((bf16[512,256]{1,0:T(8,128)(2,1)}), bf16[512,4096]{1,0:T(8,128)(2,1)}) %all-gather.20.cloned.1.call-update) | async-done | bytes 4194320 | tf_op jit(solution)/shard_map/all_gather | solution.py:226
  390.3 5.9 %fusion.5 = bf16[128,4096]{1,0:T(8,128)(2,1)} fusion(bf16[512,4096]{1,0:T(8,128)(2,1)} %all-gather.20.cloned.1.call-done, bf16[512,4096]{1,0:T(8,128)(2,1)} %all-gather.18.cloned.1.call-done, bf16[128,512]{1,0:T(8,128)(2,1)S(1)} %copy.76, bf16[128,512]{1,0:T(8,128)(2,1)S(1)} %fusion.35), kind=kOutput, calls=%fused_computation.7 | convolution fusion | flops 1091567616 | bytes 9699328 | tf_op jit(solution)/shard_map/dot_general | solution.py:231
  396.2 6.7 %reduce-scatter.2.cloned.1.call-done = bf16[64,4096]{1,0:T(8,128)(2,1)} async-done(((bf16[128,4096]{1,0:T(8,128)(2,1)}), bf16[64,4096]{1,0:T(8,128)(2,1)}) %reduce-scatter.2.cloned.1.call-update) | async-done | bytes 524304 | tf_op jit(solution)/shard_map/reduce_scatter | solution.py:230
  (96 shorter events, 14.6 us)
Async XLA Ops:
  6.5 206.2 %copy-start = (bf16[4,256,256]{2,1,0:T(8,128)(2,1)S(1)}, bf16[4,256,256]{2,1,0:T(8,128)(2,1)}, u32[]{:S(2)}) copy-start(bf16[4,256,256]{2,1,0:T(8,128)(2,1)} %param.23) | copy-start | bytes 1572868
  6.5 80.5 %copy-start.8 = (u32[32]{0:T(128)S(1)}, u32[32]{0:T(128)}, u32[]{:S(2)}) copy-start(u32[32]{0:T(128)} %constant.126) | copy-start | bytes 388
  6.5 74.2 %copy-start.2 = (bf16[256,512]{1,0:T(8,128)(2,1)S(1)}, bf16[256,512]{1,0:T(8,128)(2,1)}, u32[]{:S(2)}) copy-start(bf16[256,512]{1,0:T(8,128)(2,1)} %param.19) | copy-start | bytes 786436
  6.5 82.0 %copy-start.5 = (f32[2]{0:T(128)S(1)}, f32[2]{0:T(128)}, u32[]{:S(2)}) copy-start(f32[2]{0:T(128)} %param.25) | copy-start | bytes 28
  6.5 121.7 %all-gather.16.cloned.1.call-start = ((), (), s32[]{:S(2)}) async-start(), calls=%async_computation.12 | async-start | bytes 1310720 | tf_op jit(solution)/shard_map/all_gather | solution.py:163
  7.8 112.1 %copy-start.1 = (bf16[1,128,4096]{2,1,0:T(8,128)(2,1)S(1)}, bf16[1,128,4096]{2,1,0:T(8,128)(2,1)}, u32[]{:S(2)}) copy-start(bf16[1,128,4096]{2,1,0:T(8,128)(2,1)} %param.17) | copy-start | bytes 3145732
  7.8 112.0 %copy-start.3 = (f32[4096]{0:T(1024)S(1)}, f32[4096]{0:T(1024)}, u32[]{:S(2)}) copy-start(f32[4096]{0:T(1024)} %param.18) | copy-start | bytes 49156
  21.3 9.5 %all-to-all-start.4 = ((bf16[256,4,128]{0,2,1:T(8,128)(2,1)}), bf16[256,4,128]{0,2,1:T(8,128)(2,1)S(1)}, u32[]{:S(2)}, u32[]{:S(2)}) async-start(bf16[256,4,128]{0,2,1:T(8,128)(2,1)} %bitcast.25), calls=%async_computation.4 | async-start | bytes 524288 | tf_op jit(solution)/shard_map/all_to_all | solution.py:156
  24.7 111.4 %all-gather.14.cloned.1.call-start = ((), (), s32[]{:S(2)}) async-start(), calls=%async_computation.11 | async-start | bytes 1310720 | tf_op jit(solution)/shard_map/all_gather | solution.py:162
  28.9 24.6 %collective-permute-start = (bf16[128,4096]{1,0:T(8,128)(2,1)}, bf16[128,4096]{1,0:T(8,128)(2,1)S(1)}, u32[]{:S(2)}, u32[]{:S(2)}) collective-permute-start(bf16[128,4096]{1,0:T(8,128)(2,1)} %fusion.18), channel_id=1, source_target_pairs={{0,2},{2,4},{4,6},{6,0},{1,3},{3,5},{5,7},{7,1},{8,10},{10,12},{12... | collective-permute-start | bytes 3145736 | tf_op jit(solution)/shard_map/ppermute | solution.py:24
  31.7 113.1 %all-gather.12.cloned.1.call-start = ((), (), s32[]{:S(2)}) async-start(), calls=%async_computation.10 | async-start | bytes 1310720 | tf_op jit(solution)/shard_map/all_gather | solution.py:164
  53.5 31.6 %collective-permute-start.1 = (bf16[128,4096]{1,0:T(8,128)(2,1)S(1)}, bf16[128,4096]{1,0:T(8,128)(2,1)}, u32[]{:S(2)}, u32[]{:S(2)}) collective-permute-start(bf16[128,4096]{1,0:T(8,128)(2,1)S(1)} %collective-permute-done), channel_id=1, source_target_pairs={{0,2},{2,4},{4,6},{6,0},{1,3},{3,5},{5,7},{7,1},{8,10},{10,12},{12... | collective-permute-start | bytes 3145736 | tf_op jit(solution)/shard_map/ppermute | solution.py:24
  81.6 9.9 %all-to-all-start = ((bf16[256,4,128]{0,2,1:T(8,128)(2,1)}), bf16[256,4,128]{0,2,1:T(8,128)(2,1)S(1)}, u32[]{:S(2)}, u32[]{:S(2)}) async-start(bf16[256,4,128]{0,2,1:T(8,128)(2,1)} %bitcast.2), calls=%async_computation | async-start | bytes 524288 | tf_op jit(solution)/shard_map/all_to_all | solution.py:155
  85.0 109.6 %all-gather.10.cloned.1.call-start = ((), (), s32[]{:S(2)}) async-start(), calls=%async_computation.9 | async-start | bytes 1310720 | tf_op jit(solution)/shard_map/all_gather | solution.py:161
  85.1 29.0 %collective-permute-start.2 = (bf16[128,4096]{1,0:T(8,128)(2,1)}, bf16[128,4096]{1,0:T(8,128)(2,1)}, u32[]{:S(2)}, u32[]{:S(2)}) collective-permute-start(bf16[128,4096]{1,0:T(8,128)(2,1)} %collective-permute-done.1), channel_id=1, source_target_pairs={{0,2},{2,4},{4,6},{6,0},{1,3},{3,5},{5,7},{7,1},{8,10},{10,12},{12... | collective-permute-start | bytes 3145736 | tf_op jit(solution)/shard_map/ppermute | solution.py:24
  132.7 8.3 %all-to-all-start.7 = ((bf16[4,128,128]{1,2,0:T(8,128)(2,1)}), bf16[4,128,128]{1,2,0:T(8,128)(2,1)S(1)}, u32[]{:S(2)}, u32[]{:S(2)}) async-start(bf16[4,128,128]{1,2,0:T(8,128)(2,1)} %copy.65), calls=%async_computation.7 | async-start | bytes 262144 | tf_op jit(solution)/shard_map/all_to_all | solution.py:172
  136.1 37.5 %copy-start.7 = (f32[1024]{0:T(1024)S(1)}, f32[1024]{0:T(1024)}, u32[]{:S(2)}) copy-start(f32[1024]{0:T(1024)} %param.24) | copy-start | bytes 12292
  136.1 37.5 %copy-start.6 = (s32[4]{0:T(128)S(1)}, s32[4]{0:T(128)}, u32[]{:S(2)}) copy-start(s32[4]{0:T(128)} %constant.121.clone) | copy-start | bytes 52
  136.1 38.2 %copy-start.4 = (f32[1,2,64,256]{3,2,1,0:T(8,128)S(1)}, f32[1,2,64,256]{3,2,1,0:T(8,128)}, u32[]{:S(2)}) copy-start(f32[1,2,64,256]{3,2,1,0:T(8,128)} %param.26) | copy-start | bytes 393220
  141.0 8.8 %all-to-all-start.5 = ((bf16[4,128,128]{1,2,0:T(8,128)(2,1)}), bf16[4,128,128]{1,2,0:T(8,128)(2,1)S(1)}, u32[]{:S(2)}, u32[]{:S(2)}) async-start(bf16[4,128,128]{1,2,0:T(8,128)(2,1)} %copy.60), calls=%async_computation.5 | async-start | bytes 262144 | tf_op jit(solution)/shard_map/all_to_all | solution.py:172
  149.8 8.6 %all-to-all-start.3 = ((bf16[4,128,128]{2,1,0:T(8,128)(2,1)}), bf16[4,128,128]{2,1,0:T(8,128)(2,1)S(1)}, u32[]{:S(2)}, u32[]{:S(2)}) async-start(bf16[4,128,128]{2,1,0:T(8,128)(2,1)} %bitcast.22), calls=%async_computation.3 | async-start | bytes 262144 | tf_op jit(solution)/shard_map/all_to_all | solution.py:172
  153.5 59.9 %all-gather.22.cloned.1.call-start = ((), (), s32[]{:S(2)}) async-start(), calls=%async_computation.16 | async-start | bytes 2621440 | tf_op jit(solution)/shard_map/all_gather | solution.py:43
  160.0 142.6 %all-gather.18.cloned.1.call-start = ((), (), s32[]{:S(2)}) async-start(), calls=%async_computation.13 | async-start | bytes 4456448 | tf_op jit(solution)/shard_map/all_gather | solution.py:225
  160.6 229.7 %all-gather.20.cloned.1.call-start = ((), (), s32[]{:S(2)}) async-start(), calls=%async_computation.14 | async-start | bytes 4456448 | tf_op jit(solution)/shard_map/all_gather | solution.py:226
  199.2 8.3 %all-to-all-start.1 = ((bf16[4,128,128]{1,2,0:T(8,128)(2,1)}), bf16[4,128,128]{1,2,0:T(8,128)(2,1)S(1)}, u32[]{:S(2)}, u32[]{:S(2)}) async-start(bf16[4,128,128]{1,2,0:T(8,128)(2,1)} %copy.52), calls=%async_computation.1 | async-start | bytes 262144 | tf_op jit(solution)/shard_map/all_to_all | solution.py:172
  202.5 200.4 %reduce-scatter.2.cloned.1.call-start = ((), (), s32[]{:S(2)}) async-start(), calls=%async_computation.15 | async-start | bytes 1572864 | tf_op jit(solution)/shard_map/reduce_scatter | solution.py:230
  207.7 3.5 collective-permute-start.3
Sparse Core Ops, SparseCore 0:
  19.6 27.6 all-gather.15
  48.9 27.3 all-gather.13
  80.9 28.2 all-gather.11
  110.6 27.3 all-gather.9
  160.1 52.6 all-gather.21
  215.4 87.1 all-gather.17
  305.3 84.9 all-gather.19
  396.3 6.5 reduce-scatter.1
